TPU v7x, 32 devices: a whole 2x2x4 slice. The times are simulated.
32 devices in a mesh: fs: 8 (over z, x), tp: 4 (over y, core).
Axes of the slice: x: 2, y: 2, z: 4, core: 2. Of those that a mesh axis runs over, the one named last changes fastest.
Arguments:
- layer_input: bfloat16 [6144, 2048], P('fs'), may hold values from -6 to 6
- branch_cotangent: bfloat16 [6144, 1024], P('fs', 'tp'), may hold values from -0.057373047 to 0.057373047
- gate_cotangent: bfloat16 [6144, 1024], P('fs', 'tp'), may hold values from -0.057373047 to 0.057373047
- branch_factor: bfloat16 [2048, 128], P('fs'), may hold values from -0.5 to 0.5
- gate_factor: bfloat16 [2048, 128], P('fs'), may hold values from -0.5 to 0.5
- branch_weight: float32 [2048, 1024], P('fs', 'tp'), may hold values from -6 to 6
- gate_weight: float32 [2048, 1024], P('fs', 'tp'), may hold values from -6 to 6
- branch_first: float32 [128, 1024], P(None, 'tp'), may hold values from -6 to 6
- gate_first: float32 [128, 1024], P(None, 'tp'), may hold values from -6 to 6
- branch_second: float32 [128, 1024], P(None, 'tp'), may hold values from 0.0625 to 900
- gate_second: float32 [128, 1024], P(None, 'tp'), may hold values from 0.0625 to 900
Outputs:
- branch_step: float32 [2048, 1024], P('fs', 'tp')
- gate_step: float32 [2048, 1024], P('fs', 'tp')
- branch_new: float32 [2048, 1024], P('fs', 'tp')
- gate_new: float32 [2048, 1024], P('fs', 'tp')
- branch_copy: bfloat16 [2048, 1024], P(None, 'tp')
- gate_copy: bfloat16 [2048, 1024], P(None, 'tp')
- branch_first_new: float32 [128, 1024], P(None, 'tp')
- gate_first_new: float32 [128, 1024], P(None, 'tp')
- branch_second_new: float32 [128, 1024], P(None, 'tp')
- gate_second_new: float32 [128, 1024], P(None, 'tp')
All inputs are finite; a program needn't handle non-finite values.
Results may differ from a plain program's by a relative error of at most 0.00055.
Values may be sent and summed in bfloat16 or wider, within the bound.
A program may use at most 64 MiB of HBM per device.

v0:
```python
import jax
import jax.numpy as jnp
from jax import lax
from jax.sharding import PartitionSpec as P

first_decay = 0.8
second_decay = 0.9
learn_rate = 0.5


def update_moments(projected, first_old, second_old):
    first_new = first_decay * first_old + (1.0 - first_decay) * projected
    second_new = second_decay * second_old + (1.0 - second_decay) * projected * projected
    return (first_new, second_new, first_new / jnp.sqrt(second_new))


def local(
    layer_input,
    branch_cotangent,
    gate_cotangent,
    branch_factor,
    gate_factor,
    branch_weight,
    gate_weight,
    branch_first,
    gate_first,
    branch_second,
    gate_second,
):
    highest = lax.Precision.HIGHEST
    width = branch_cotangent.shape[1]
    branch_whole, gate_whole = (
        lax.all_gather(branch_factor, "fs", axis=0, tiled=True),
        lax.all_gather(gate_factor, "fs", axis=0, tiled=True),
    )
    branch_rows = jnp.dot(layer_input, branch_whole, preferred_element_type=jnp.float32)
    gate_rows = jnp.dot(layer_input, gate_whole, preferred_element_type=jnp.float32)
    branch_local = jnp.einsum(
        "tr,tw->rw", branch_rows, branch_cotangent.astype(jnp.float32), precision=highest
    )
    gate_local = jnp.einsum(
        "tr,tw->rw", gate_rows, gate_cotangent.astype(jnp.float32), precision=highest
    )
    branch_projected, gate_projected = lax.psum((branch_local, gate_local), "fs")
    branch_first_new, branch_second_new, branch_direction = update_moments(
        branch_projected, branch_first, branch_second
    )
    gate_first_new, gate_second_new, gate_direction = update_moments(
        gate_projected, gate_first, gate_second
    )
    local_squares = jnp.sum(branch_direction * branch_direction) + jnp.sum(
        gate_direction * gate_direction
    )
    sum_squares = lax.psum(local_squares, "tp")
    entries = 2 * branch_direction.shape[0] * width * lax.axis_size("tp")
    step_scale = learn_rate / jnp.sqrt(sum_squares / entries + 1e-06)
    branch_step = -step_scale * jnp.dot(
        branch_factor.astype(jnp.float32), branch_direction, precision=highest
    )
    gate_step = -step_scale * jnp.dot(
        gate_factor.astype(jnp.float32), gate_direction, precision=highest
    )
    branch_new = branch_weight + branch_step
    gate_new = gate_weight + gate_step
    branch_copy, gate_copy = (
        lax.all_gather(branch_new.astype(jnp.bfloat16), "fs", axis=0, tiled=True),
        lax.all_gather(gate_new.astype(jnp.bfloat16), "fs", axis=0, tiled=True),
    )
    return (
        branch_step,
        gate_step,
        branch_new,
        gate_new,
        branch_copy,
        gate_copy,
        branch_first_new,
        gate_first_new,
        branch_second_new,
        gate_second_new,
    )


def solution(mesh):
    return jax.shard_map(
        local,
        mesh=mesh,
        in_specs=(
            P("fs", None),
            P("fs", "tp"),
            P("fs", "tp"),
            P("fs", None),
            P("fs", None),
            P("fs", "tp"),
            P("fs", "tp"),
            P(None, "tp"),
            P(None, "tp"),
            P(None, "tp"),
            P(None, "tp"),
        ),
        out_specs=(
            P("fs", "tp"),
            P("fs", "tp"),
            P("fs", "tp"),
            P("fs", "tp"),
            P(None, "tp"),
            P(None, "tp"),
            P(None, "tp"),
            P(None, "tp"),
            P(None, "tp"),
            P(None, "tp"),
        ),
        check_vma=False,
    )
```

profile of v0, /device:TPU:0, one launch (start us, length us, event | category | flops | bytes accessed | tf_op | source)
XLA Modules:
  0.0 251.8 jit_solution(14178861783154490260)
XLA Ops:
  7.2 0.0 copy-start
  7.2 0.0 all-reduce.3.cloned.1.call-start
  7.2 33.4 %all_gather.12 = bf16[2048,128]{1,0:T(8,128)(2,1)S(1)} all-gather(bf16[256,128]{1,0:T(8,128)(2,1)} %param.14), channel_id=1, replica_groups=mesh['fs'=8,'tp'=4] {'fs'}, dimensions={0}, use_global_device_ids=true | all-gather | bytes 589824 | tf_op jit(solution)/shard_map/all_gather | solution.py:33
  40.6 31.4 %all_gather.13 = bf16[2048,128]{1,0:T(8,128)(2,1)S(1)} all-gather(bf16[256,128]{1,0:T(8,128)(2,1)} %param.15), channel_id=1, replica_groups=mesh['fs'=8,'tp'=4] {'fs'}, dimensions={0}, use_global_device_ids=true | all-gather | bytes 589824 | tf_op jit(solution)/shard_map/all_gather | solution.py:34
  72.0 0.0 copy-done
  72.0 1.0 fusion.8
  73.0 0.0 copy-start.2
  73.0 0.0 copy-start.3
  73.0 0.0 copy-start.4
  73.0 1.0 fusion.10
  74.0 0.0 copy-done.2
  74.0 1.1 fusion.9
  75.2 0.0 copy-done.3
  75.2 1.1 fusion.11
  76.3 0.0 all-reduce.3.cloned.1.call-update
  76.3 0.0 all-gather.5.cloned.1.call-start
  76.4 72.8 %all-reduce.3.cloned.1.call-done = (f32[128,256]{1,0:T(8,128)}, f32[128,256]{1,0:T(8,128)}) async-done(((f32[128,256]{1,0:T(8,128)}, f32[128,256]{1,0:T(8,128)}), (f32[128,256]{1,0:T(8,128)}, f32[128,256]{1,0:T(8,128)})) %all-reduce.3.cloned.1.call-update) | async-done | bytes 262160 | tf_op jit(solution)/shard_map/psum | solution.py:44
  149.1 2.6 %multiply_reduce_fusion = (f32[]{:T(128)}, f32[128,256]{1,0:T(8,128)S(1)}, f32[128,256]{1,0:T(8,128)}, f32[]{:T(128)}, f32[128,256]{1,0:T(8,128)}, /*index=5*/f32[128,256]{1,0:T(8,128)}) fusion(f32[128,256]{1,0:T(8,128)} %get-tuple-element.21, f32[128,256]{1,0:T(8,128)} %param.21, f32[128,256]{1,0:T(8,128)} %param.19, f32[128,256]{1,0:T(8,128)} %get-tuple-element.20, ...), kind=kLoop, calls=%fused_computation.8 | loop fusion | flops 655358 | bytes 1310728 | tf_op jit(solution)/shard_map/reduce_sum | solution.py:51
  151.7 0.0 copy-start.1
  153.0 0.0 copy-done.4
  153.1 0.8 copy.22
  153.9 6.1 %psum.23 = f32[]{:T(128)} all-reduce(f32[]{:T(128)S(6)} %add.34), channel_id=1, replica_groups=mesh['fs'=8,'tp'=4] {'tp'}, use_global_device_ids=true, to_apply=%region_4.0 | all-reduce | flops 1 | bytes 8 | tf_op jit(solution)/shard_map/psum | solution.py:54
  160.7 2.1 fusion.4
  162.8 0.0 all-gather.5.cloned.1.call-update
  162.9 0.0 all-gather.3.cloned.1.call-start
  162.9 1.8 copy.21
  164.7 2.3 fusion.5
  167.0 0.0 all-gather.3.cloned.1.call-update
  167.0 1.8 copy.26
  168.8 0.8 copy.24
  169.6 1.8 copy.25
  171.4 1.8 copy.23
  173.2 28.7 %all-gather.5.cloned.1.call-done = bf16[2048,256]{0,1:T(8,128)(2,1)} async-done(((bf16[256,256]{0,1:T(8,128)(2,1)}), bf16[2048,256]{0,1:T(8,128)(2,1)}) %all-gather.5.cloned.1.call-update) | async-done | bytes 1048592 | tf_op jit(solution)/shard_map/all_gather | solution.py:67
  201.9 2.3 copy.28
  204.2 0.0 copy-done.1
  204.2 38.8 %all-gather.3.cloned.1.call-done = bf16[2048,256]{0,1:T(8,128)(2,1)} async-done(((bf16[256,256]{0,1:T(8,128)(2,1)}), bf16[2048,256]{0,1:T(8,128)(2,1)}) %all-gather.3.cloned.1.call-update) | async-done | bytes 1048592 | tf_op jit(solution)/shard_map/all_gather | solution.py:66
  243.0 2.3 copy.27
Async XLA Ops:
  7.2 64.8 %copy-start = (bf16[768,2048]{1,0:T(8,128)(2,1)S(1)}, bf16[768,2048]{1,0:T(8,128)(2,1)}, u32[]{:S(2)}) copy-start(bf16[768,2048]{1,0:T(8,128)(2,1)} %param.11) | copy-start | bytes 9437188
  7.2 142.0 %all-reduce.3.cloned.1.call-start = ((), (), s32[]{:S(2)}) async-start(), calls=%async_computation.2 | async-start | bytes 524288 | tf_op jit(solution)/shard_map/psum | solution.py:44
  73.0 1.0 copy-start.2
  73.0 2.2 copy-start.3
  73.0 80.0 %copy-start.4 = (f32[256,256]{1,0:T(8,128)S(1)}, f32[256,256]{1,0:T(8,128)}, u32[]{:S(2)}) copy-start(f32[256,256]{1,0:T(8,128)} %param.17) | copy-start | bytes 786436
  76.3 125.6 %all-gather.5.cloned.1.call-start = ((), (), s32[]{:S(2)}) async-start(), calls=%async_computation.1 | async-start | bytes 1179648 | tf_op jit(solution)/shard_map/all_gather | solution.py:67
  151.7 52.4 %copy-start.1 = (f32[128,256]{1,0:T(8,128)}, f32[128,256]{1,0:T(8,128)S(1)}, u32[]{:S(2)}) copy-start(f32[128,256]{1,0:T(8,128)S(1)} %get-tuple-element.27) | copy-start | bytes 393220
  162.9 80.1 %all-gather.3.cloned.1.call-start = ((), (), s32[]{:S(2)}) async-start(), calls=%async_computation | async-start | bytes 1179648 | tf_op jit(solution)/shard_map/all_gather | solution.py:66
Sparse Core Ops, SparseCore 0:
  76.5 72.6 all-reduce.2
  163.0 38.8 all-gather.4
  204.5 38.3 all-gather.2
where the time goes:
time: 252 us
  waiting for transfers between devices  140 us (56%)
  blocking collectives  70.9 us (28%)
  between operations  15.8 us (6%)
  local copies, waits for them, and re-layouts  13.4 us (5%)
  matrix products  8.61 us (3%)
  other arithmetic  2.6 us (1%)
    psum x1, waiting for transfers between devices, local(): lax.psum((branch_local, gate_local), 'fs')  72.8 us
    all_gather x1, waiting for transfers between devices, local(): lax.all_gather(branch_new.astype(jnp.bfloat16), 'fs', axis=0, tiled=True)  38.8 us
    all_gather x1, blocking collectives, local(): lax.all_gather(branch_factor, 'fs', axis=0, tiled=True)  33.4 us
    all_gather x1, blocking collectives, local(): lax.all_gather(gate_factor, 'fs', axis=0, tiled=True)  31.4 us
    all_gather x1, waiting for transfers between devices, local(): lax.all_gather(gate_new.astype(jnp.bfloat16), 'fs', axis=0, tiled=True)  28.7 us
    unnamed x18, local copies, waits for them, and re-layouts  13.4 us
    psum x1, blocking collectives, local(): sum_squares = lax.psum(local_squares, 'tp')  6.14 us
  transfers between devices with their start and end apart: 3, of which 3 were waited for; matrix products, arithmetic and copies ran while one was open for 5% of the time, Pallas kernels for 0%

commit v1 on v0

--- a/solution.py
+++ b/solution.py
@@ -30,7 +30,9 @@
     highest = lax.Precision.HIGHEST
     width = branch_cotangent.shape[1]
     branch_whole, gate_whole = (
-        lax.all_gather(branch_factor, "fs", axis=0, tiled=True),
+        jnp.concatenate(
+            lax.all_to_all(jnp.stack([branch_factor] * lax.axis_size("fs")), "fs", 0, 0), axis=0
+        ),
         lax.all_gather(gate_factor, "fs", axis=0, tiled=True),
     )
     branch_rows = jnp.dot(layer_input, branch_whole, preferred_element_type=jnp.float32)

time: 252 us -> 233 us (0.925)
  blocking collectives: 70.9 us -> 44.7 us
  starting transfers between devices: 0.12 us -> 7.41 us
  waiting for transfers between devices: 140 us -> 136 us
  local copies, waits for them, and re-layouts: 13.4 us -> 16.2 us
    all_gather x1 -> x0, blocking collectives: 33.4 us -> none  [local(): lax.all_gather(branch_factor, 'fs', axis=0, tiled=True)]
    all_to_all x0 -> x1, starting transfers between devices: none -> 7.28 us  [local(): lax.all_to_all(jnp.stack([branch_factor] * lax.axis_size('fs')), 'fs', 0, 0)]
    all_gather x1, blocking collectives: 31.4 us -> 38.5 us  [local(): lax.all_gather(gate_factor, 'fs', axis=0, tiled=True)]
    psum x1, waiting for transfers between devices: 72.8 us -> 68.7 us  [local(): lax.psum((branch_local, gate_local), 'fs')]
    unnamed x18 -> x16, local copies, waits for them, and re-layouts: 13.4 us -> 14.3 us
  transfers between devices with their start and end apart: 3 -> 4, of which waited for: 3 -> 3; matrix products, arithmetic and copies ran while one was open for 5% -> 6% of each run, Pallas kernels for 0% -> 0%
where the time goes in v1:
time: 233 us
  waiting for transfers between devices  136 us (58%)
  blocking collectives  44.7 us (19%)
  local copies, waits for them, and re-layouts  16.2 us (7%)
  between operations  15.8 us (7%)
  matrix products  9.71 us (4%)
  starting transfers between devices  7.41 us (3%)
  other arithmetic  2.6 us (1%)
    psum x1, waiting for transfers between devices, local(): lax.psum((branch_local, gate_local), 'fs')  68.7 us
    all_gather x1, waiting for transfers between devices, local(): lax.all_gather(branch_new.astype(jnp.bfloat16), 'fs', axis=0, tiled=True)  38.8 us
    all_gather x1, blocking collectives, local(): lax.all_gather(gate_factor, 'fs', axis=0, tiled=True)  38.5 us
    all_gather x1, waiting for transfers between devices, local(): lax.all_gather(gate_new.astype(jnp.bfloat16), 'fs', axis=0, tiled=True)  28.7 us
    unnamed x16, local copies, waits for them, and re-layouts  14.3 us
    all_to_all x1, starting transfers between devices, local(): lax.all_to_all(jnp.stack([branch_factor] * lax.axis_size('fs')), 'fs', 0, 0)  7.28 us
    psum x1, blocking collectives, local(): sum_squares = lax.psum(local_squares, 'tp')  6.14 us
  transfers between devices with their start and end apart: 4, of which 3 were waited for; matrix products, arithmetic and copies ran while one was open for 6% of the time, Pallas kernels for 0%

profile of v1, /device:TPU:0, one launch (start us, length us, event | category | flops | bytes accessed | tf_op | source)
XLA Modules:
  0.0 232.6 jit_solution(5471260114349986773)
XLA Ops:
  7.2 0.0 copy-start
  7.2 1.9 stack.2
  9.0 7.3 %all-to-all-start = ((bf16[8,256,128]{2,1,0:T(8,128)(2,1)}), bf16[8,256,128]{2,1,0:T(8,128)(2,1)}, u32[]{:S(2)}, u32[]{:S(2)}) async-start(bf16[8,256,128]{2,1,0:T(8,128)(2,1)} %stack.2), calls=%async_computation | async-start | bytes 1048576 | tf_op jit(solution)/shard_map/all_to_all | solution.py:34
  16.3 0.0 copy-start.2
  16.3 0.0 all-reduce.3.cloned.1.call-start
  16.4 38.5 %all_gather.9 = bf16[2048,128]{1,0:T(8,128)(2,1)S(1)} all-gather(bf16[256,128]{1,0:T(8,128)(2,1)} %param.15), channel_id=1, replica_groups=mesh['fs'=8,'tp'=4] {'fs'}, dimensions={0}, use_global_device_ids=true | all-gather | bytes 589824 | tf_op jit(solution)/shard_map/all_gather | solution.py:36
  54.9 0.0 copy-done
  54.9 1.0 fusion.10
  55.9 0.0 copy-done.2
  55.9 1.1 fusion.11
  57.1 0.0 copy-start.3
  57.1 0.0 all-to-all-done
  57.1 2.1 fusion.8
  59.1 0.0 copy-done.3
  59.1 1.1 fusion.9
  60.3 0.0 all-reduce.3.cloned.1.call-update
  60.3 0.0 all-gather.5.cloned.1.call-start
  60.3 68.7 %all-reduce.3.cloned.1.call-done = (f32[128,256]{1,0:T(8,128)}, f32[128,256]{1,0:T(8,128)}) async-done(((f32[128,256]{1,0:T(8,128)}, f32[128,256]{1,0:T(8,128)}), (f32[128,256]{1,0:T(8,128)}, f32[128,256]{1,0:T(8,128)})) %all-reduce.3.cloned.1.call-update) | async-done | bytes 262160 | tf_op jit(solution)/shard_map/psum | solution.py:46
  129.1 2.6 %multiply_reduce_fusion = (f32[]{:T(128)}, f32[128,256]{1,0:T(8,128)S(1)}, f32[128,256]{1,0:T(8,128)}, f32[]{:T(128)}, f32[128,256]{1,0:T(8,128)}, /*index=5*/f32[128,256]{1,0:T(8,128)}) fusion(f32[128,256]{1,0:T(8,128)} %get-tuple-element.21, f32[128,256]{1,0:T(8,128)} %param.21, f32[128,256]{1,0:T(8,128)} %param.19, f32[128,256]{1,0:T(8,128)} %get-tuple-element.20, ...), kind=kLoop, calls=%fused_computation.8 | loop fusion | flops 655358 | bytes 1310728 | tf_op jit(solution)/shard_map/reduce_sum | solution.py:53
  131.7 0.0 copy-start.1
  133.0 1.8 copy.22
  134.7 6.1 %psum.23 = f32[]{:T(128)} all-reduce(f32[]{:T(128)S(6)} %add.34), channel_id=1, replica_groups=mesh['fs'=8,'tp'=4] {'tp'}, use_global_device_ids=true, to_apply=%region_4.0 | all-reduce | flops 1 | bytes 8 | tf_op jit(solution)/shard_map/psum | solution.py:56
  141.6 2.1 fusion.4
  143.7 0.0 all-gather.5.cloned.1.call-update
  143.7 0.0 all-gather.3.cloned.1.call-start
  143.8 1.8 copy.21
  145.6 2.3 fusion.5
  147.8 0.0 all-gather.3.cloned.1.call-update
  147.8 1.8 copy.26
  149.6 0.8 copy.24
  150.5 1.8 copy.25
  152.3 1.8 copy.23
  154.1 28.7 %all-gather.5.cloned.1.call-done = bf16[2048,256]{0,1:T(8,128)(2,1)} async-done(((bf16[256,256]{0,1:T(8,128)(2,1)}), bf16[2048,256]{0,1:T(8,128)(2,1)}) %all-gather.5.cloned.1.call-update) | async-done | bytes 1048592 | tf_op jit(solution)/shard_map/all_gather | solution.py:69
  182.8 2.3 copy.28
  185.0 0.0 copy-done.1
  185.0 38.8 %all-gather.3.cloned.1.call-done = bf16[2048,256]{0,1:T(8,128)(2,1)} async-done(((bf16[256,256]{0,1:T(8,128)(2,1)}), bf16[2048,256]{0,1:T(8,128)(2,1)}) %all-gather.3.cloned.1.call-update) | async-done | bytes 1048592 | tf_op jit(solution)/shard_map/all_gather | solution.py:68
  223.8 2.3 copy.27
Async XLA Ops:
  7.2 47.7 %copy-start = (bf16[768,2048]{1,0:T(8,128)(2,1)S(1)}, bf16[768,2048]{1,0:T(8,128)(2,1)}, u32[]{:S(2)}) copy-start(bf16[768,2048]{1,0:T(8,128)(2,1)} %param.11) | copy-start | bytes 9437188
  9.0 48.0 %all-to-all-start = ((bf16[8,256,128]{2,1,0:T(8,128)(2,1)}), bf16[8,256,128]{2,1,0:T(8,128)(2,1)}, u32[]{:S(2)}, u32[]{:S(2)}) async-start(bf16[8,256,128]{2,1,0:T(8,128)(2,1)} %stack.2), calls=%async_computation | async-start | bytes 1048576 | tf_op jit(solution)/shard_map/all_to_all | solution.py:34
  16.3 39.6 %copy-start.2 = (bf16[768,256]{1,0:T(8,128)(2,1)S(1)}, bf16[768,256]{1,0:T(8,128)(2,1)}, u32[]{:S(2)}) copy-start(bf16[768,256]{1,0:T(8,128)(2,1)} %param.13) | copy-start | bytes 1179652
  16.3 112.7 %all-reduce.3.cloned.1.call-start = ((), (), s32[]{:S(2)}) async-start(), calls=%async_computation.3 | async-start | bytes 524288 | tf_op jit(solution)/shard_map/psum | solution.py:46
  57.1 2.1 copy-start.3
  60.3 122.5 %all-gather.5.cloned.1.call-start = ((), (), s32[]{:S(2)}) async-start(), calls=%async_computation.2 | async-start | bytes 1179648 | tf_op jit(solution)/shard_map/all_gather | solution.py:69
  131.7 53.4 %copy-start.1 = (f32[128,256]{1,0:T(8,128)}, f32[128,256]{1,0:T(8,128)S(1)}, u32[]{:S(2)}) copy-start(f32[128,256]{1,0:T(8,128)S(1)} %get-tuple-element.27) | copy-start | bytes 393220
  143.7 80.1 %all-gather.3.cloned.1.call-start = ((), (), s32[]{:S(2)}) async-start(), calls=%async_computation.1 | async-start | bytes 1179648 | tf_op jit(solution)/shard_map/all_gather | solution.py:68
Sparse Core Ops, SparseCore 0:
  60.4 68.5 all-reduce.2
  143.8 38.8 all-gather.4
  185.4 38.3 all-gather.2
